TPU v7x, 512 devices: a whole 4x4x16 slice. The times are simulated.
512 devices in a mesh: ep: 128 (over z, x, core), tp: 4 (over y).
Axes of the slice: x: 4, y: 4, z: 16, core: 2. Of those that a mesh axis runs over, the one named last changes fastest.
Arguments:
- tokens: bfloat16 [1024, 1024], P('ep'), may hold values from -6 to 6
- lengths: int32 [1024], P('ep'), may hold values from 1 to 512, as said below
- cache_keys: bfloat16 [1024, 512, 4, 128], P('ep', None, 'tp'), may hold values from -2.5 to 2.5
- cache_values: bfloat16 [1024, 512, 4, 128], P('ep', None, 'tp'), may hold values from -6 to 6
- cache_cum: float32 [1024, 4, 512], P('ep', 'tp'), may hold values from -1536 to 0, as said below
- norm_gain: bfloat16 [1024], replicated, may hold values from 0.099609375 to 1.8984375
- query_weight: bfloat16 [1024, 1024], P(None, 'tp'), may hold values from -0.1875 to 0.1875
- key_weight: bfloat16 [1024, 512], P(None, 'tp'), may hold values from -0.1875 to 0.1875
- value_weight: bfloat16 [1024, 512], P(None, 'tp'), may hold values from -0.1875 to 0.1875
- forget_weight: bfloat16 [1024, 4], P(None, 'tp'), may hold values from -0.1875 to 0.1875
- forget_bias: float32 [4], P('tp'), may hold values from -1 to 2
- query_gain: bfloat16 [128], replicated, may hold values from 0.29882812 to 2.5
- key_gain: bfloat16 [128], replicated, may hold values from 0.099609375 to 1.8984375
- out_weight: bfloat16 [1024, 1024], P('tp'), may hold values from -0.1875 to 0.1875
- ffn_gain: bfloat16 [1024], replicated, may hold values from 0.099609375 to 1.8984375
- mix_weight: bfloat16 [1024], replicated, may hold values from -0.1875 to 0.1875
- shared_gate: bfloat16 [1024, 4096], P(None, 'ep'), may hold values from -0.1875 to 0.1875
- shared_up: bfloat16 [1024, 4096], P(None, 'ep'), may hold values from -0.1875 to 0.1875
- shared_down: bfloat16 [4096, 1024], P('ep', 'tp'), may hold values from -0.09375 to 0.09375
- routes: int32 [1024, 2], P('ep'), may hold values from 0 to 127, all different within a row; in each aligned block of 8 rows (0 to 7, 8 to 15, ...) at most 4 rows name the same one
- route_weights: float32 [1024, 2], P('ep'), may hold values from 0.1 to 1
- expert_gate: bfloat16 [128, 1024, 512], P('ep', None, 'tp'), may hold values from -0.1875 to 0.1875
- expert_up: bfloat16 [128, 1024, 512], P('ep', None, 'tp'), may hold values from -0.1875 to 0.1875
- expert_down: bfloat16 [128, 512, 1024], P('ep', 'tp'), may hold values from -0.25 to 0.25
Outputs:
- layer_out: bfloat16 [1024, 1024], P('ep', 'tp')
Inputs may be any that keep to these rules, and one draw needn't show every extreme that they name: `lengths`: at least one sequence has exactly 512 cached positions. `cache_cum`: along the positions each row never rises. `routes`: the 2 experts of a token differ; among the 8 rows of one device no expert is named by more than 4 rows, a bound that some block reaches.
All inputs are finite; a program needn't handle non-finite values.
Results may differ from a plain program's by a relative error of at most 0.013.
Values may be sent and summed in bfloat16 or wider, within the bound.
A program may use at most 64 MiB of HBM per device.

v0:
```python
import functools

import jax
import jax.numpy as jnp
from jax import lax
from jax.experimental import pallas as pl
from jax.experimental.pallas import tpu as pltpu
from jax.sharding import Mesh
from jax.sharding import PartitionSpec as P

MESH = pl.DeviceIdType.MESH
EP = ("z", "x", "c")
EPS = 1e-06
META = 128
BF = jnp.bfloat16
NG = 2
F32 = jnp.float32


def rms(values, gain):
    return values * lax.rsqrt(jnp.mean(values * values, axis=-1, keepdims=True) + EPS) * gain


def row_of(ref):
    return ref[...].astype(F32).reshape(1, -1)


def nt(a, b):
    return lax.dot_general(a, b, (((1,), (1,)), ((), ())), preferred_element_type=F32)


def mm(a, b):
    return jnp.dot(a, b, preferred_element_type=F32)


def silu(v):
    return v / (1.0 + jnp.exp(-v))


class Phases:
    def __init__(self):
        self.open = None

    def __call__(self, name):
        self.close()
        self.open = jax.named_scope(name)
        self.open.__enter__()

    def close(self):
        if self.open is not None:
            self.open.__exit__(None, None, None)
            self.open = None


def hi_lo(v):
    hi = v.astype(BF).astype(F32)
    return hi, (v - hi).astype(BF).astype(F32)


def kernel(
    dims,
    tokens_h, lengths_h, cum_h, norm_gain_h, forget_w_h, forget_b_h, query_gain_h, key_gain_h, ffn_gain_h,
    mix_w_h, routes_h, route_w_h,
    keys_h, values_h, qw_h, kw_h, vw_h, ow_h, sg_h, su_h, sd_h, eg_h, eu_h, ed_h,
    out,
    tokens, lengths, cum, norm_gain, forget_w, forget_b, query_gain, key_gain, ffn_gain, mix_w,
    routes, route_w,
    keys, values, wqkv, ow, sg, su, wsd, wgu, wd,
    pt, zb, g, p3, rx1, s1, rx2, zs, rx3,
    known, lsem, wsend, wrecv, tsend, trecv, zsend, zrecv, xsend, xrecv, csend, crecv, ysend, yrecv,
    c2send, c2recv, x2send, x2recv, z2send, z2recv,
):
    nz, nx, nc, nt_ = dims
    phase = Phases()
    z, x, c, t = (lax.axis_index(a) for a in ("z", "x", "c", "t"))
    batch, depth = tokens.shape
    rows = batch // nt_
    head = keys.shape[2]
    cache = keys.shape[1]
    groups = qw_h.shape[1] // head
    width = depth // nt_
    hidden = eg_h.shape[1]
    wide = depth + META
    near = nz // NG
    strip = near * rows
    part_rows = nx * 2 * strip
    order = sorted(range(nz), key=lambda d: (min(d, nz - d), d))
    place = [order.index(d) for d in range(nz)]

    def idx(base, step, size):
        return lax.rem(base + (step % size), size)

    def at(axis, base, step, size):
        return {axis: idx(base, step, size)}

    def rcopy(src, dst, ss, rs, dev):
        return pltpu.make_async_remote_copy(
            src_ref=src, dst_ref=dst, send_sem=ss, recv_sem=rs, device_id=dev, device_id_type=MESH
        )

    def send(*args):
        rcopy(*args).start()

    def landed(ref, sem):
        pltpu.make_async_copy(ref, ref, sem).wait()

    phase("entry")
    barrier = pltpu.get_barrier_semaphore()
    partners = (
        [at("t", t, d, nt_) for d in range(1, nt_)]
        + [at("c", c, d, nc) for d in range(1, nc)]
        + [at("x", x, d, nx) for d in range(1, nx)]
        + [at("z", z, d, nz) for d in range(1, nz) if min(d, nz - d) <= nz // 4]
    )
    for dev in partners:
        pl.semaphore_signal(barrier, inc=1, device_id=dev, device_id_type=MESH)

    def local(i, src, dst):
        return pltpu.make_async_copy(src, dst, lsem.at[i])

    nq, nk = qw_h.shape[1], kw_h.shape[1]
    loads = [
        local(0, qw_h, wqkv.at[:, 0:nq]),
        local(0, kw_h, wqkv.at[:, nq : nq + nk]),
        local(0, vw_h, wqkv.at[:, nq + nk : nq + 2 * nk]),
        local(3, keys_h, keys),
        local(4, values_h, values),
        local(5, ow_h, ow),
        local(6, eg_h, wgu.at[0, :, 0:hidden]),
        local(6, eu_h, wgu.at[0, :, hidden : 2 * hidden]),
        local(8, ed_h, wd.at[0]),
        local(9, sd_h, wsd.at[t]),
        local(10, sg_h, sg),
        local(11, su_h, su),
    ]
    small = [
        local(12 + i, src, dst)
        for i, (src, dst) in enumerate((
            (tokens_h, tokens), (norm_gain_h, norm_gain), (forget_w_h, forget_w), (forget_b_h, forget_b),
            (query_gain_h, query_gain), (key_gain_h, key_gain), (lengths_h, lengths), (cum_h, cum),
            (ffn_gain_h, ffn_gain), (mix_w_h, mix_w), (routes_h, routes), (route_w_h, route_w),
        ))
    ]
    for cp in small + loads:
        cp.start()
    phase("small_wait")
    for cp in small:
        cp.wait()

    opp = idx(t, 2, nt_)
    partner = lax.rem(t + 1 + 2 * lax.rem(t + c, 2), nt_)
    wsd[opp] = jnp.zeros(wsd.shape[1:], BF)
    wsd[idx(partner, 2, nt_)] = jnp.zeros(wsd.shape[1:], BF)

    phase("norm")
    tok = tokens[...].astype(F32)
    normed = rms(tok, row_of(norm_gain)).astype(BF)
    logit = jnp.sum(normed.astype(F32) * forget_w[...].astype(F32), axis=-1, keepdims=True) + forget_b[...]
    new_log = jnp.minimum(logit, 0.0) - jnp.log(1.0 + jnp.exp(-jnp.abs(logit)))
    landed(wqkv, lsem.at[0])
    phase("qkv")
    qkv = mm(normed, wqkv[...])
    qg, kg = row_of(query_gain), row_of(key_gain)
    q16 = jnp.concatenate(
        [rms(qkv[:, i * head : (i + 1) * head], qg).astype(BF) for i in range(groups)], axis=0
    )
    new_key = rms(qkv[:, nq : nq + nk], kg).astype(BF).astype(F32)
    new_value = qkv[:, nq + nk : nq + 2 * nk].astype(BF).astype(F32)
    new_key = jnp.concatenate([new_key] * groups, axis=0)
    new_value = jnp.concatenate([new_value] * groups, axis=0)
    phase("bias")
    n16 = batch * groups
    row16 = lax.rem(lax.broadcasted_iota(jnp.int32, (n16, cache), 0), batch)
    row8 = lax.broadcasted_iota(jnp.int32, (batch, cache), 0)
    pos8 = lax.broadcasted_iota(jnp.int32, (batch, cache), 1)
    length8 = jnp.zeros((batch, cache), jnp.int32)
    cum8 = jnp.zeros((batch, cache), F32)
    for s in range(batch):
        length8 = jnp.where(row8 == s, lengths[s], length8)
        cum8 = jnp.where(row8 == s, cum[s], cum8)
    last = jnp.sum(jnp.where(pos8 == length8 - 1, cum8, 0.0), axis=-1, keepdims=True)
    bias8 = last - cum8 + new_log
    bias8 = jnp.where(pos8 < length8, bias8, -jnp.inf)
    bias16 = jnp.concatenate([bias8] * groups, axis=0)
    loads[3].wait()
    phase("scores")
    scores = jnp.zeros((n16, cache), F32)
    for s in range(batch):
        scores = jnp.where(row16 == s, nt(q16, keys[s]), scores)
    phase("softmax")
    scale = head ** (-0.5)
    past = jnp.exp(scores * scale + bias16)
    own = jnp.exp(jnp.sum(q16.astype(F32) * new_key, axis=-1, keepdims=True) * scale)
    denominator = jnp.sum(past, axis=-1, keepdims=True) + own
    prob = (past / denominator).astype(BF).astype(F32)
    own_prob = (own / denominator).astype(BF).astype(F32)
    loads[4].wait()
    phase("values")
    mixed = own_prob * new_value
    for s in range(batch):
        mixed = mixed + mm(jnp.where(row16 == s, prob, 0.0).astype(BF), values[s])
    mixed = mixed.astype(BF)
    loads[5].wait()
    phase("outproj")
    heads = jnp.concatenate([mixed[i * batch : (i + 1) * batch] for i in range(groups)], axis=1)
    partial = mm(heads, ow[...]).astype(BF)
    pt[0] = partial

    phase("barrier")
    pl.semaphore_wait(barrier, len(partners))
    for d in (nz // 4, nz - nz // 4):
        pl.semaphore_signal(known, inc=1, device_id=at("z", z, d, nz), device_id_type=MESH)
    phase("tsend")
    for d in (2, 1, 3):
        send(pt.at[0], pt.at[d], tsend, trecv, at("t", t, d, nt_))

    landed(wgu.at[0], lsem.at[6])
    loads[8].wait()
    loads[9].wait()
    there = {"t": partner}
    send(wgu.at[0], wgu.at[1], wsend.at[0], wrecv.at[0], there)
    send(wd.at[0], wd.at[1], wsend.at[1], wrecv.at[1], there)
    send(wsd.at[t], wsd.at[t], wsend.at[2], wrecv.at[2], there)

    phase("route")
    rowm = lax.broadcasted_iota(jnp.int32, (batch, META), 0)
    lane = lax.broadcasted_iota(jnp.int32, (batch, META), 1)
    zero = jnp.zeros((batch, META), F32)
    r0, r1, w0, w1 = zero, zero, zero, zero
    for s in range(batch):
        here = rowm == s
        r0 = jnp.where(here, routes[0, s].astype(F32), r0)
        r1 = jnp.where(here, routes[1, s].astype(F32), r1)
        w0 = jnp.where(here, route_w[0, s], w0)
        w1 = jnp.where(here, route_w[1, s], w1)
    total = w0 + w1
    h0, l0 = hi_lo(w0 / total)
    h1, l1 = hi_lo(w1 / total)
    for i in (10, 11):
        loads[i].wait()

    phase("twait")
    landed(pt.at[1:nt_], trecv)
    residual = tok + pt[0].astype(F32)
    for d in range(1, nt_):
        residual = residual + pt[d].astype(F32)
    phase("ffn")
    ffn = rms(residual, row_of(ffn_gain)).astype(BF).astype(F32)
    gate = jnp.sum(ffn * row_of(mix_w), axis=-1, keepdims=True)
    gate = 1.0 / (1.0 + jnp.exp(-gate))
    hg, lg = hi_lo(jnp.broadcast_to(gate, (batch, META)))
    meta = zero
    for i, v in enumerate((r0, r1, h0, l0, h1, l1, hg, lg)):
        meta = jnp.where(lane == i, v, meta)
    full = jnp.concatenate([ffn, meta], axis=1)
    sel = full[0:rows]
    for k in range(1, nt_):
        sel = jnp.where(t == k, full[k * rows : (k + 1) * rows], sel)
    zb[0] = sel.astype(BF)
    mine8 = residual[:, 0:width]
    for k in range(1, nt_):
        mine8 = jnp.where(t == k, residual[:, k * width : (k + 1) * width], mine8)

    phase("spread2")
    pl.semaphore_wait(known, 2)
    phase("zsend")
    for d in order[:0:-1]:
        send(zb.at[0], zb.at[place[d]], zsend, zrecv.at[place[d] // near], at("z", z, d, nz))

    twin = {"c": 1 - c}
    level = lax.div(t, 2)

    def spot(dx, dq):
        return 2 * idx(x, dx, nx) + (1 - level if dq else level)

    def place_of(dx, dq):
        return {"x": idx(x, dx, nx), "t": idx(t, 2 * dq, nt_)}

    far_first = [(2, 1), (2, 0), (1, 1), (3, 1), (0, 1), (1, 0), (3, 0)]
    me = spot(0, 0)

    def take_z(h):
        phase("zwait#h=%d" % h)
        landed(zb.at[max(1, h * near) : (h + 1) * near], zrecv.at[h])
        phase("xsend#h=%d" % h)
        g[h, c, me] = zb[h * near : (h + 1) * near].reshape(strip, wide)
        piece = g.at[h, c, me]
        send(piece, piece, ysend, yrecv.at[h], {"t": opp})
        hand_on(h, 0)

    def hand_on(h, dq):
        piece = g.at[h, c, spot(0, dq)]
        for dx in (2, 1, 3):
            send(piece, piece, xsend.at[h], xrecv.at[h, dq, dx], at("x", x, dx, nx))
        send(piece, piece, csend.at[h], crecv.at[h], twin)

    def take_y(h):
        phase("yfwd#h=%d" % h)
        landed(g.at[h, c, spot(0, 1)], yrecv.at[h])
        hand_on(h, 1)

    def take_x(h, dq):
        phase("xwait%d#h=%d" % (dq, h))
        for dx in (1, 3, 2):
            piece = g.at[h, c, spot(nx - dx, dq)]
            landed(piece, xrecv.at[h, dq, dx])
            send(piece, piece, csend.at[h], crecv.at[h], twin)

    def take_c(h):
        phase("cwait#h=%d" % h)
        landed(g.at[h, 1 - c], crecv.at[h])

    mine = ((z * nx + x) * nc + c).astype(F32)

    def compute(h, core, name):
        phase("%s#h=%d" % (name, h))
        every = g[h, core].reshape(part_rows, wide)
        info = every[:, depth:wide].astype(F32)
        w = jnp.where(info[:, 0:1] == mine, info[:, 2:3] + info[:, 3:4], 0.0)
        w = w + jnp.where(info[:, 1:2] == mine, info[:, 4:5] + info[:, 5:6], 0.0)
        xs = every[:, 0:depth]
        hid = []
        for k in (0, 1):
            pre = mm(xs, wgu[k])
            hid.append((silu(pre[:, 0:hidden]) * pre[:, hidden : 2 * hidden]).astype(BF))
        sh = (silu(nt(xs, sg[...])) * nt(xs, su[...])).astype(BF)
        dense = jnp.concatenate([mm(sh, wsd[k]) for k in range(nt_)], axis=1)
        res = mm(jnp.concatenate(hid, axis=1), wd[...].reshape(2 * hidden, depth))
        value = w * res + (info[:, 6:7] + info[:, 7:8]) * dense
        p3[h, core] = value.astype(BF).reshape(2 * nx, strip, depth)

    def send_c(h):
        send(p3.at[h, 1 - c], rx1.at[h], c2send.at[h], c2recv.at[h], twin)

    def sum_c(h):
        phase("c2#h=%d" % h)
        landed(rx1.at[h], c2recv.at[h])
        for dx, dq in far_first:
            at_ = spot(dx, dq)
            s1[h, at_] = (p3[h, c, at_].astype(F32) + rx1[h, at_].astype(F32)).astype(BF)
            send(s1.at[h, at_], rx2.at[h, 2 * dx + dq], x2send.at[h], x2recv.at[h], place_of(dx, dq))

    def sum_x(h):
        phase("x2#h=%d" % h)
        acc = p3[h, c, me].astype(F32) + rx1[h, me].astype(F32)
        landed(rx2.at[h, 1 : 2 * nx], x2recv.at[h])
        for i in range(1, 2 * nx):
            acc = acc + rx2[h, i].astype(F32)
        phase("z2send#h=%d" % h)
        for k in range(nt_):
            zs[h, k * near : (k + 1) * near] = acc[:, k * width : (k + 1) * width].astype(BF).reshape(near, rows, width)
        for d in order[h * near : (h + 1) * near][::-1]:
            i = place[d] - h * near
            for e in (2, 1, 3, 0):
                if d or e:
                    peer = idx(t, e, nt_)
                    send(zs.at[h, peer * near + i], rx3.at[t, d], z2send.at[h], z2recv.at[t], {"z": idx(z, nz - d, nz), "t": peer})
                else:
                    rx3[t, 0] = zs[0, t * near]

    take_z(0)
    take_z(1)
    take_y(0)
    take_x(0, 0)
    take_y(1)
    take_x(0, 1)
    phase("wwait")
    landed(wgu.at[1], wrecv.at[0])
    landed(wd.at[1], wrecv.at[1])
    landed(wsd.at[partner], wrecv.at[2])
    compute(0, c, "own")
    take_x(1, 0)
    take_c(0)
    compute(0, 1 - c, "twin")
    send_c(0)
    take_x(1, 1)
    compute(1, c, "own")
    sum_c(0)
    take_c(1)
    compute(1, 1 - c, "twin")
    send_c(1)
    sum_c(NG - 1)
    for h in range(NG):
        sum_x(h)
    phase("z2wait")
    for e in range(nt_):
        k = idx(t, e, nt_)
        landed(rx3.at[k] if e else rx3.at[k, 1:nz], z2recv.at[k])
    phase("result")
    sums = [jnp.sum(rx3[k].astype(F32), axis=0) for k in range(nt_)]
    out[...] = mine8 + jnp.concatenate(sums, axis=0)

    phase("drain")
    landed(pt.at[1:nt_], tsend)
    landed(zb.at[1:nz], zsend)
    landed(wgu.at[0], wsend.at[0])
    landed(wd.at[0], wsend.at[1])
    landed(wsd.at[0], wsend.at[2])
    landed(g.at[0, 0, 0:NG], ysend)
    for h in range(NG):
        landed(g.at[h, 0, 2 : 2 * nx], xsend.at[h])
        landed(g.at[h, 0], csend.at[h])
        landed(rx1.at[h], c2send.at[h])
        landed(rx2.at[h, 1 : 2 * nx], x2send.at[h])
        landed(zs.at[h] if h else zs.at[h, 1 : nt_ * near], z2send.at[h])
    phase.close()


def per_device(
    dims, tokens, lengths, cache_keys, cache_values, cache_cum, norm_gain, query_weight, key_weight,
    value_weight, forget_weight, forget_bias, query_gain, key_gain, out_weight, ffn_gain, mix_weight,
    shared_gate, shared_up, shared_down, routes, route_weights, expert_gate, expert_up, expert_down,
):
    nz, nx, nc, ny = dims
    batch, depth = tokens.shape
    cache, head = cache_keys.shape[1], cache_keys.shape[3]
    rows = batch // ny
    width = depth // ny
    strip = nz // NG * rows
    hidden = expert_gate.shape[2]
    nq, nk = query_weight.shape[1], key_weight.shape[1]
    fs = shared_gate.shape[1]
    vm = pl.BlockSpec(memory_space=pltpu.VMEM)
    hb = pl.BlockSpec(memory_space=pltpu.HBM)
    dma = pltpu.SemaphoreType.DMA
    scratch = [
        pltpu.VMEM((batch, depth), BF),
        pltpu.SMEM((batch,), jnp.int32),
        pltpu.VMEM((batch, 1, cache), F32),
        pltpu.VMEM((depth,), BF),
        pltpu.VMEM((1, depth), BF),
        pltpu.VMEM((1, 1), F32),
        pltpu.VMEM((head,), BF),
        pltpu.VMEM((head,), BF),
        pltpu.VMEM((depth,), BF),
        pltpu.VMEM((depth,), BF),
        pltpu.SMEM((routes.shape[1], batch), jnp.int32),
        pltpu.SMEM((routes.shape[1], batch), F32),
        pltpu.VMEM((batch, cache, head), BF),
        pltpu.VMEM((batch, cache, head), BF),
        pltpu.VMEM((depth, nq + 2 * nk), BF),
        pltpu.VMEM((nq, depth), BF),
        pltpu.VMEM((fs, depth), BF),
        pltpu.VMEM((fs, depth), BF),
        pltpu.VMEM((ny, fs, width), BF),
        pltpu.VMEM((2, depth, 2 * hidden), BF),
        pltpu.VMEM((2, hidden, depth), BF),
        pltpu.VMEM((ny, batch, depth), BF),
        pltpu.VMEM((nz, rows, depth + META), BF),
        pltpu.VMEM((NG, nc, 2 * nx, strip, depth + META), BF),
        pltpu.VMEM((NG, nc, 2 * nx, strip, depth), BF),
        pltpu.VMEM((NG, 2 * nx, strip, depth), BF),
        pltpu.VMEM((NG, 2 * nx, strip, depth), BF),
        pltpu.VMEM((NG, 2 * nx, strip, depth), BF),
        pltpu.VMEM((NG, ny * (nz // NG), rows, width), BF),
        pltpu.VMEM((ny, nz, rows, width), BF),
        pltpu.SemaphoreType.REGULAR,
        dma((24,)),
        dma((3,)), dma((3,)),
        dma, dma, dma, dma((NG,)), dma((NG,)), dma((NG, 2, nx)), dma((NG,)), dma((NG,)), dma, dma((NG,)),
        dma((NG,)), dma((NG,)), dma((NG,)), dma((NG,)), dma((NG,)), dma((ny,)),
    ]
    return pl.pallas_call(
        functools.partial(kernel, dims),
        out_shape=jax.ShapeDtypeStruct((batch, width), F32),
        in_specs=[hb] * 24,
        out_specs=vm,
        scratch_shapes=scratch,
        compiler_params=pltpu.CompilerParams(
            collective_id=0, has_side_effects=True, vmem_limit_bytes=60 * 1024 * 1024
        ),
    )(
        tokens, lengths, cache_cum, norm_gain, forget_weight.T, forget_bias.reshape(1, 1), query_gain, key_gain,
        ffn_gain, mix_weight, routes.T, route_weights.T,
        cache_keys.reshape(batch, cache, head), cache_values.reshape(batch, cache, head),
        query_weight, key_weight, value_weight, out_weight, shared_gate.T, shared_up.T, shared_down,
        expert_gate[0], expert_up[0], expert_down[0],
    ).astype(BF)


def solution(mesh):
    ep, ny = mesh.shape["ep"], mesh.shape["tp"]
    nz, nx, nc = (16, 4, 2) if ep == 128 else (ep // 4, 2, 2)
    finer = Mesh(mesh.devices.reshape(nz, nx, nc, ny), ("z", "x", "c", "t"))
    placed = (
        P(EP, None),
        P(EP),
        P(EP, None, "t", None),
        P(EP, None, "t", None),
        P(EP, "t", None),
        P(),
        P(None, "t"),
        P(None, "t"),
        P(None, "t"),
        P(None, "t"),
        P("t"),
        P(),
        P(),
        P("t", None),
        P(),
        P(),
        P(None, EP),
        P(None, EP),
        P(EP, "t"),
        P(EP, None),
        P(EP, None),
        P(EP, None, "t"),
        P(EP, None, "t"),
        P(EP, "t", None),
    )
    return jax.shard_map(
        functools.partial(per_device, (nz, nx, nc, ny)),
        mesh=finer, in_specs=placed, out_specs=P(EP, "t"), check_vma=False,
    )
```

profile of v0, /device:TPU:1, one launch (start us, length us, event | category | flops | bytes accessed | tf_op | source)
XLA Modules:
  0.0 54.7 jit_solution(5014685344141661272)
XLA Ops:
  0.7 52.8 %shard_map.226 = f32[8,256]{1,0:T(8,128)} custom-call(bf16[8,1024]{1,0:T(8,128)(2,1)} %tokens_h.1, s32[8]{0:T(128)} %lengths_h.1, f32[8,1,512]{2,1,0:T(1,128)} %cum_h.1, bf16[1024]{0:T(1024)(128)(2,1)} %norm_gain_h.1, bf16[1,1024]{1,0:T(2,128)(2,1)} %bitcast.19, f32[1,1]{1,0:T(1,128)} %bitcast.11.forget_b_h, bf16[128]{0:T(256)(128)(2,1)} %query_gain_h.1, ...), custom_call_target="tpu_custom_call" | custom-call | tf_op jit(solution)/shard_map/pallas_call | solution.py:463
  53.5 1.3 %convert_element_type.3 = bf16[8,256]{1,0:T(8,128)(2,1)} convert(f32[8,256]{1,0:T(8,128)} %shard_map.226) | non-fusion elementwise | flops 2048 | bytes 12288 | tf_op jit(solution)/shard_map/convert_element_type | solution.py:478
where the time goes:
time: 55 us; the launch traced here: 54.7 us
  Pallas kernels  52.8 us (96%)
  other arithmetic  1.29 us (2%)
  between operations  0.66 us (1%)
    pallas_call x1, Pallas kernels, per_device(): pl.pallas_call(functools.partial(kernel, dims), out_shape=jax.ShapeDtypeS...  52.8 us
    convert_element_type x1, other arithmetic, per_device(): return pl.pallas_call(functools.partial(kernel, dims), out_shape=jax.Shap...  1.29 us

commit v1 on v0

--- a/solution.py
+++ b/solution.py
@@ -13,7 +13,7 @@
 EPS = 1e-06
 META = 128
 BF = jnp.bfloat16
-NG = 2
+NG = 4
 F32 = jnp.float32
 
 
@@ -66,7 +66,7 @@
     tokens, lengths, cum, norm_gain, forget_w, forget_b, query_gain, key_gain, ffn_gain, mix_w,
     routes, route_w,
     keys, values, wqkv, ow, sg, su, wsd, wgu, wd,
-    pt, zb, g, p3, rx1, s1, rx2, zs, rx3,
+    pt, ob, zb, g, p3, rx1, s1, rx2, zs, rx3,
     known, lsem, wsend, wrecv, tsend, trecv, zsend, zrecv, xsend, xrecv, csend, crecv, ysend, yrecv,
     c2send, c2recv, x2send, x2recv, z2send, z2recv,
 ):
@@ -84,9 +84,6 @@
     near = nz // NG
     strip = near * rows
     part_rows = nx * 2 * strip
-    order = sorted(range(nz), key=lambda d: (min(d, nz - d), d))
-    place = [order.index(d) for d in range(nz)]
-
     def idx(base, step, size):
         return lax.rem(base + (step % size), size)
 
@@ -256,16 +253,27 @@
     sel = full[0:rows]
     for k in range(1, nt_):
         sel = jnp.where(t == k, full[k * rows : (k + 1) * rows], sel)
-    zb[0] = sel.astype(BF)
+    ob[0] = sel.astype(BF)
     mine8 = residual[:, 0:width]
     for k in range(1, nt_):
         mine8 = jnp.where(t == k, residual[:, k * width : (k + 1) * width], mine8)
 
+    group = lax.div(z, near)
+
+    def give_z(d):
+        send(ob.at[0], zb.at[z], zsend, zrecv.at[group], at("z", z, d, nz))
+
+    phase("zsend")
+    pltpu.make_async_copy(ob.at[0], zb.at[z], zrecv.at[group]).start()
+    by_distance = sorted(range(1, nz), key=lambda d: (-min(d, nz - d), d))
+    for d in by_distance:
+        if min(d, nz - d) <= nz // 4:
+            give_z(d)
     phase("spread2")
     pl.semaphore_wait(known, 2)
-    phase("zsend")
-    for d in order[:0:-1]:
-        send(zb.at[0], zb.at[place[d]], zsend, zrecv.at[place[d] // near], at("z", z, d, nz))
+    for d in by_distance:
+        if min(d, nz - d) > nz // 4:
+            give_z(d)
 
     twin = {"c": 1 - c}
     level = lax.div(t, 2)
@@ -281,7 +289,7 @@
 
     def take_z(h):
         phase("zwait#h=%d" % h)
-        landed(zb.at[max(1, h * near) : (h + 1) * near], zrecv.at[h])
+        landed(zb.at[h * near : (h + 1) * near], zrecv.at[h])
         phase("xsend#h=%d" % h)
         g[h, c, me] = zb[h * near : (h + 1) * near].reshape(strip, wide)
         piece = g.at[h, c, me]
@@ -291,7 +299,7 @@
     def hand_on(h, dq):
         piece = g.at[h, c, spot(0, dq)]
         for dx in (2, 1, 3):
-            send(piece, piece, xsend.at[h], xrecv.at[h, dq, dx], at("x", x, dx, nx))
+            send(piece, piece, xsend.at[h], xrecv.at[h, dq], at("x", x, dx, nx))
         send(piece, piece, csend.at[h], crecv.at[h], twin)
 
     def take_y(h):
@@ -301,9 +309,9 @@
 
     def take_x(h, dq):
         phase("xwait%d#h=%d" % (dq, h))
-        for dx in (1, 3, 2):
-            piece = g.at[h, c, spot(nx - dx, dq)]
-            landed(piece, xrecv.at[h, dq, dx])
+        landed(g.at[h, c, 0 : nx - 1], xrecv.at[h, dq])
+        for dx in range(1, nx):
+            piece = g.at[h, c, spot(dx, dq)]
             send(piece, piece, csend.at[h], crecv.at[h], twin)
 
     def take_c(h):
@@ -312,9 +320,9 @@
 
     mine = ((z * nx + x) * nc + c).astype(F32)
 
-    def compute(h, core, name):
-        phase("%s#h=%d" % (name, h))
-        every = g[h, core].reshape(part_rows, wide)
+    def compute(h):
+        phase("compute#h=%d" % h)
+        every = g[h].reshape(nc * part_rows, wide)
         info = every[:, depth:wide].astype(F32)
         w = jnp.where(info[:, 0:1] == mine, info[:, 2:3] + info[:, 3:4], 0.0)
         w = w + jnp.where(info[:, 1:2] == mine, info[:, 4:5] + info[:, 5:6], 0.0)
@@ -327,7 +335,8 @@
         dense = jnp.concatenate([mm(sh, wsd[k]) for k in range(nt_)], axis=1)
         res = mm(jnp.concatenate(hid, axis=1), wd[...].reshape(2 * hidden, depth))
         value = w * res + (info[:, 6:7] + info[:, 7:8]) * dense
-        p3[h, core] = value.astype(BF).reshape(2 * nx, strip, depth)
+        p3[h] = value.astype(BF).reshape(nc, 2 * nx, strip, depth)
+        send_c(h)
 
     def send_c(h):
         send(p3.at[h, 1 - c], rx1.at[h], c2send.at[h], c2recv.at[h], twin)
@@ -347,45 +356,61 @@
         for i in range(1, 2 * nx):
             acc = acc + rx2[h, i].astype(F32)
         phase("z2send#h=%d" % h)
+        base = h * nt_ * near
         for k in range(nt_):
-            zs[h, k * near : (k + 1) * near] = acc[:, k * width : (k + 1) * width].astype(BF).reshape(near, rows, width)
-        for d in order[h * near : (h + 1) * near][::-1]:
-            i = place[d] - h * near
+            zs[base + k * near : base + (k + 1) * near] = (
+                acc[:, k * width : (k + 1) * width].astype(BF).reshape(near, rows, width)
+            )
+
+        def give(i, e):
+            there = lax.rem(z + i, near) + h * near
+            peer = idx(t, e, nt_)
+            piece = zs.at[base + peer * near + there - h * near]
+
+            def remote():
+                send(piece, rx3.at[t, z], z2send, z2recv.at[t], {"z": there, "t": peer})
+
+            if i or e:
+                remote()
+            else:
+                pl.when(there != z)(remote)
+                pl.when(there == z)(lambda: pltpu.make_async_copy(piece, rx3.at[t, z], z2recv.at[t]).start())
+
+        for i in range(near):
             for e in (2, 1, 3, 0):
-                if d or e:
-                    peer = idx(t, e, nt_)
-                    send(zs.at[h, peer * near + i], rx3.at[t, d], z2send.at[h], z2recv.at[t], {"z": idx(z, nz - d, nz), "t": peer})
-                else:
-                    rx3[t, 0] = zs[0, t * near]
-
-    take_z(0)
-    take_z(1)
-    take_y(0)
-    take_x(0, 0)
-    take_y(1)
-    take_x(0, 1)
+                give(i, e)
+
+    for h in range(NG):
+        take_z(h)
+    for h in range(NG):
+        take_y(h)
+        take_x(h, 0)
     phase("wwait")
     landed(wgu.at[1], wrecv.at[0])
     landed(wd.at[1], wrecv.at[1])
     landed(wsd.at[partner], wrecv.at[2])
-    compute(0, c, "own")
-    take_x(1, 0)
+    take_x(0, 1)
+    take_x(1, 1)
     take_c(0)
-    compute(0, 1 - c, "twin")
-    send_c(0)
-    take_x(1, 1)
-    compute(1, c, "own")
+    compute(0)
+    take_x(2, 1)
+    take_c(1)
+    compute(1)
     sum_c(0)
-    take_c(1)
-    compute(1, 1 - c, "twin")
-    send_c(1)
-    sum_c(NG - 1)
+    take_x(3, 1)
+    take_c(2)
+    compute(2)
+    sum_c(1)
+    take_c(3)
+    compute(3)
+    sum_c(2)
+    sum_c(3)
     for h in range(NG):
         sum_x(h)
     phase("z2wait")
     for e in range(nt_):
         k = idx(t, e, nt_)
-        landed(rx3.at[k] if e else rx3.at[k, 1:nz], z2recv.at[k])
+        landed(rx3.at[k], z2recv.at[k])
     phase("result")
     sums = [jnp.sum(rx3[k].astype(F32), axis=0) for k in range(nt_)]
     out[...] = mine8 + jnp.concatenate(sums, axis=0)
@@ -397,12 +422,12 @@
     landed(wd.at[0], wsend.at[1])
     landed(wsd.at[0], wsend.at[2])
     landed(g.at[0, 0, 0:NG], ysend)
+    landed(zs.at[1 : nt_ * nz], z2send)
     for h in range(NG):
         landed(g.at[h, 0, 2 : 2 * nx], xsend.at[h])
         landed(g.at[h, 0], csend.at[h])
         landed(rx1.at[h], c2send.at[h])
         landed(rx2.at[h, 1 : 2 * nx], x2send.at[h])
-        landed(zs.at[h] if h else zs.at[h, 1 : nt_ * near], z2send.at[h])
     phase.close()
 
 
@@ -446,19 +471,20 @@
         pltpu.VMEM((2, depth, 2 * hidden), BF),
         pltpu.VMEM((2, hidden, depth), BF),
         pltpu.VMEM((ny, batch, depth), BF),
+        pltpu.VMEM((1, rows, depth + META), BF),
         pltpu.VMEM((nz, rows, depth + META), BF),
         pltpu.VMEM((NG, nc, 2 * nx, strip, depth + META), BF),
         pltpu.VMEM((NG, nc, 2 * nx, strip, depth), BF),
         pltpu.VMEM((NG, 2 * nx, strip, depth), BF),
         pltpu.VMEM((NG, 2 * nx, strip, depth), BF),
         pltpu.VMEM((NG, 2 * nx, strip, depth), BF),
-        pltpu.VMEM((NG, ny * (nz // NG), rows, width), BF),
+        pltpu.VMEM((ny * nz, rows, width), BF),
         pltpu.VMEM((ny, nz, rows, width), BF),
         pltpu.SemaphoreType.REGULAR,
         dma((24,)),
         dma((3,)), dma((3,)),
-        dma, dma, dma, dma((NG,)), dma((NG,)), dma((NG, 2, nx)), dma((NG,)), dma((NG,)), dma, dma((NG,)),
-        dma((NG,)), dma((NG,)), dma((NG,)), dma((NG,)), dma((NG,)), dma((ny,)),
+        dma, dma, dma, dma((NG,)), dma((NG,)), dma((NG, 2)), dma((NG,)), dma((NG,)), dma, dma((NG,)),
+        dma((NG,)), dma((NG,)), dma((NG,)), dma((NG,)), dma, dma((ny,)),
     ]
     return pl.pallas_call(
         functools.partial(kernel, dims),

time: 55 us -> 51.4 us (0.935)
  Pallas kernels: 52.8 us -> 48.8 us
    pallas_call x1, Pallas kernels: 52.8 us -> 48.8 us  [per_device(): pl.pallas_call(functools.partial(kernel, dims), out_shape=jax.ShapeDtypeS...]
where the time goes in v1:
time: 51.4 us; the launch traced here: 50.8 us
  Pallas kernels  48.8 us (95%)
  other arithmetic  1.29 us (3%)
  between operations  0.66 us (1%)
    pallas_call x1, Pallas kernels, per_device(): pl.pallas_call(functools.partial(kernel, dims), out_shape=jax.ShapeDtypeS...  48.8 us
    convert_element_type x1, other arithmetic, per_device(): return pl.pallas_call(functools.partial(kernel, dims), out_shape=jax.Shap...  1.29 us

profile of v1, /device:TPU:1, one launch (start us, length us, event | category | flops | bytes accessed | tf_op | source)
XLA Modules:
  0.0 50.8 jit_solution(1152798677924453690)
XLA Ops:
  0.7 48.8 %shard_map.226 = f32[8,256]{1,0:T(8,128)} custom-call(bf16[8,1024]{1,0:T(8,128)(2,1)} %tokens_h.1, s32[8]{0:T(128)} %lengths_h.1, f32[8,1,512]{2,1,0:T(1,128)} %cum_h.1, bf16[1024]{0:T(1024)(128)(2,1)} %norm_gain_h.1, bf16[1,1024]{1,0:T(2,128)(2,1)} %bitcast.19, f32[1,1]{1,0:T(1,128)} %bitcast.11.forget_b_h, bf16[128]{0:T(256)(128)(2,1)} %query_gain_h.1, ...), custom_call_target="tpu_custom_call" | custom-call | tf_op jit(solution)/shard_map/pallas_call | solution.py:489
  49.5 1.3 %convert_element_type.3 = bf16[8,256]{1,0:T(8,128)(2,1)} convert(f32[8,256]{1,0:T(8,128)} %shard_map.226) | non-fusion elementwise | flops 2048 | bytes 12288 | tf_op jit(solution)/shard_map/convert_element_type | solution.py:504

commit v2 on v1

--- a/solution.py
+++ b/solution.py
@@ -66,7 +66,7 @@
     tokens, lengths, cum, norm_gain, forget_w, forget_b, query_gain, key_gain, ffn_gain, mix_w,
     routes, route_w,
     keys, values, wqkv, ow, sg, su, wsd, wgu, wd,
-    pt, ob, zb, g, p3, rx1, s1, rx2, zs, rx3,
+    pt, ob, za, zb, g, p3, rx1, s1, rx2, zs, rx3,
     known, lsem, wsend, wrecv, tsend, trecv, zsend, zrecv, xsend, xrecv, csend, crecv, ysend, yrecv,
     c2send, c2recv, x2send, x2recv, z2send, z2recv,
 ):
@@ -107,10 +107,19 @@
         [at("t", t, d, nt_) for d in range(1, nt_)]
         + [at("c", c, d, nc) for d in range(1, nc)]
         + [at("x", x, d, nx) for d in range(1, nx)]
-        + [at("z", z, d, nz) for d in range(1, nz) if min(d, nz - d) <= nz // 4]
     )
+    along = [d for d in range(1, nz) if min(d, nz - d) <= nz // 4]
+
+    def tell_z(sem, steps, cores):
+        @pl.when(c == 1)
+        def _():
+            for d in steps:
+                for core in cores:
+                    pl.semaphore_signal(sem, inc=1, device_id={**at("z", z, d, nz), "c": core}, device_id_type=MESH)
+
     for dev in partners:
         pl.semaphore_signal(barrier, inc=1, device_id=dev, device_id_type=MESH)
+    tell_z(barrier, along, (0, 1))
 
     def local(i, src, dst):
         return pltpu.make_async_copy(src, dst, lsem.at[i])
@@ -204,9 +213,8 @@
     pt[0] = partial
 
     phase("barrier")
-    pl.semaphore_wait(barrier, len(partners))
-    for d in (nz // 4, nz - nz // 4):
-        pl.semaphore_signal(known, inc=1, device_id=at("z", z, d, nz), device_id_type=MESH)
+    pl.semaphore_wait(barrier, len(partners) + len(along))
+    tell_z(known, (nz // 4, nz - nz // 4), (1,))
     phase("tsend")
     for d in (2, 1, 3):
         send(pt.at[0], pt.at[d], tsend, trecv, at("t", t, d, nt_))
@@ -250,33 +258,53 @@
     for i, v in enumerate((r0, r1, h0, l0, h1, l1, hg, lg)):
         meta = jnp.where(lane == i, v, meta)
     full = jnp.concatenate([ffn, meta], axis=1)
-    sel = full[0:rows]
-    for k in range(1, nt_):
-        sel = jnp.where(t == k, full[k * rows : (k + 1) * rows], sel)
-    ob[0] = sel.astype(BF)
+    parity, level = lax.rem(t, 2), lax.div(t, 2)
+    for q in (0, 1):
+        lo = 2 * q * rows
+        ob[q] = jnp.where(parity == 1, full[lo + rows : lo + 2 * rows], full[lo : lo + rows]).astype(BF)
     mine8 = residual[:, 0:width]
     for k in range(1, nt_):
         mine8 = jnp.where(t == k, residual[:, k * width : (k + 1) * width], mine8)
 
     group = lax.div(z, near)
 
-    def give_z(d):
-        send(ob.at[0], zb.at[z], zsend, zrecv.at[group], at("z", z, d, nz))
+    def give_z(dev):
+        @pl.when(group == 0)
+        def _():
+            send(ob, za.at[z, c], zsend, zrecv.at[0], dev)
+
+        @pl.when(group != 0)
+        def _():
+            send(ob.at[level], zb.at[z, c], zsend, zrecv.at[group], dev)
+
+    def keep_z():
+        @pl.when(group == 0)
+        def _():
+            pltpu.make_async_copy(ob, za.at[z, 1], zrecv.at[0]).start()
+
+        @pl.when(group != 0)
+        def _():
+            pltpu.make_async_copy(ob.at[level], zb.at[z, 1], zrecv.at[group]).start()
 
     phase("zsend")
-    pltpu.make_async_copy(ob.at[0], zb.at[z], zrecv.at[group]).start()
+    pl.when(c == 0)(lambda: give_z({"c": 1}))
+    pl.when(c == 1)(keep_z)
     by_distance = sorted(range(1, nz), key=lambda d: (-min(d, nz - d), d))
     for d in by_distance:
-        if min(d, nz - d) <= nz // 4:
-            give_z(d)
+        if d in along:
+            give_z({**at("z", z, d, nz), "c": 1})
     phase("spread2")
-    pl.semaphore_wait(known, 2)
+    pl.semaphore_wait(known, 1 + c)
+
+    @pl.when(c == 1)
+    def _():
+        pl.semaphore_signal(known, inc=1, device_id={"c": 0}, device_id_type=MESH)
+
     for d in by_distance:
-        if min(d, nz - d) > nz // 4:
-            give_z(d)
+        if d not in along:
+            give_z({**at("z", z, d, nz), "c": 1})
 
     twin = {"c": 1 - c}
-    level = lax.div(t, 2)
 
     def spot(dx, dq):
         return 2 * idx(x, dx, nx) + (1 - level if dq else level)
@@ -287,38 +315,52 @@
     far_first = [(2, 1), (2, 0), (1, 1), (3, 1), (0, 1), (1, 0), (3, 0)]
     me = spot(0, 0)
 
+    def core1(f):
+        return lambda *args: pl.when(c == 1)(lambda: f(*args))
+
+    @core1
     def take_z(h):
-        phase("zwait#h=%d" % h)
-        landed(zb.at[h * near : (h + 1) * near], zrecv.at[h])
-        phase("xsend#h=%d" % h)
-        g[h, c, me] = zb[h * near : (h + 1) * near].reshape(strip, wide)
-        piece = g.at[h, c, me]
-        send(piece, piece, ysend, yrecv.at[h], {"t": opp})
-        hand_on(h, 0)
-
-    def hand_on(h, dq):
-        piece = g.at[h, c, spot(0, dq)]
+        if h == 0:
+            landed(za, zrecv.at[0])
+            for q in (0, 1):
+                for core in (0, 1):
+                    g[0, 2 * x + q, core] = za[:, core, q].reshape(strip, wide)
+            hand_on(0)
+        else:
+            landed(zb.at[h * near : (h + 1) * near], zrecv.at[h])
+            for core in (0, 1):
+                g[h, me, core] = zb[h * near : (h + 1) * near, core].reshape(strip, wide)
+            send(g.at[h, me], g.at[h, me], ysend, yrecv.at[h], {"t": opp})
+
+    def hand_on(h):
         for dx in (2, 1, 3):
-            send(piece, piece, xsend.at[h], xrecv.at[h, dq], at("x", x, dx, nx))
-        send(piece, piece, csend.at[h], crecv.at[h], twin)
-
+            for dq in (0, 1):
+                piece = g.at[h, spot(0, dq)]
+                send(piece, piece, xsend.at[h], xrecv.at[h], at("x", x, dx, nx))
+        for dq in (0, 1):
+            piece = g.at[h, spot(0, dq)]
+            send(piece, piece, csend.at[h], crecv.at[h], {"c": 0})
+
+    @core1
     def take_y(h):
-        phase("yfwd#h=%d" % h)
-        landed(g.at[h, c, spot(0, 1)], yrecv.at[h])
-        hand_on(h, 1)
-
-    def take_x(h, dq):
-        phase("xwait%d#h=%d" % (dq, h))
-        landed(g.at[h, c, 0 : nx - 1], xrecv.at[h, dq])
+        landed(g.at[h, spot(0, 1)], yrecv.at[h])
+        hand_on(h)
+
+    @core1
+    def take_x(h):
+        landed(g.at[h, 2 : 2 * nx], xrecv.at[h])
         for dx in range(1, nx):
-            piece = g.at[h, c, spot(dx, dq)]
-            send(piece, piece, csend.at[h], crecv.at[h], twin)
+            for dq in (0, 1):
+                piece = g.at[h, spot(dx, dq)]
+                send(piece, piece, csend.at[h], crecv.at[h], {"c": 0})
 
     def take_c(h):
         phase("cwait#h=%d" % h)
-        landed(g.at[h, 1 - c], crecv.at[h])
+        pl.when(c == 0)(lambda: landed(g.at[h], crecv.at[h]))
 
     mine = ((z * nx + x) * nc + c).astype(F32)
+
+    side = depth // 2
 
     def compute(h):
         phase("compute#h=%d" % h)
@@ -335,8 +377,10 @@
         dense = jnp.concatenate([mm(sh, wsd[k]) for k in range(nt_)], axis=1)
         res = mm(jnp.concatenate(hid, axis=1), wd[...].reshape(2 * hidden, depth))
         value = w * res + (info[:, 6:7] + info[:, 7:8]) * dense
-        p3[h] = value.astype(BF).reshape(nc, 2 * nx, strip, depth)
-        send_c(h)
+        value = value.reshape(2 * nx, nc, strip, depth)
+        for core in (0, 1):
+            for q in (0, 1):
+                p3[h, core, q] = value[:, core, :, q * side : (q + 1) * side].reshape(nx, 2 * strip, side).astype(BF)
 
     def send_c(h):
         send(p3.at[h, 1 - c], rx1.at[h], c2send.at[h], c2recv.at[h], twin)
@@ -345,87 +389,116 @@
         phase("c2#h=%d" % h)
         landed(rx1.at[h], c2recv.at[h])
         for dx, dq in far_first:
-            at_ = spot(dx, dq)
-            s1[h, at_] = (p3[h, c, at_].astype(F32) + rx1[h, at_].astype(F32)).astype(BF)
-            send(s1.at[h, at_], rx2.at[h, 2 * dx + dq], x2send.at[h], x2recv.at[h], place_of(dx, dq))
+            px, q = idx(x, dx, nx), 1 - level if dq else level
+            s1[h, q, px] = (p3[h, c, q, px].astype(F32) + rx1[h, q, px].astype(F32)).astype(BF)
+            send(s1.at[h, q, px], rx2.at[h, 2 * dx + dq], x2send.at[h], x2recv.at[h], place_of(dx, dq))
 
     def sum_x(h):
         phase("x2#h=%d" % h)
-        acc = p3[h, c, me].astype(F32) + rx1[h, me].astype(F32)
+        acc = p3[h, c, level, x].astype(F32) + rx1[h, level, x].astype(F32)
         landed(rx2.at[h, 1 : 2 * nx], x2recv.at[h])
         for i in range(1, 2 * nx):
             acc = acc + rx2[h, i].astype(F32)
         phase("z2send#h=%d" % h)
-        base = h * nt_ * near
-        for k in range(nt_):
-            zs[base + k * near : base + (k + 1) * near] = (
-                acc[:, k * width : (k + 1) * width].astype(BF).reshape(near, rows, width)
-            )
+        base = h * 2 * near
+        for k in (0, 1):
+            for q in (0, 1):
+                zs[base + k * near : base + (k + 1) * near, q] = (
+                    acc[q * strip : (q + 1) * strip, k * width : (k + 1) * width].astype(BF).reshape(near, rows, width)
+                )
 
         def give(i, e):
             there = lax.rem(z + i, near) + h * near
-            peer = idx(t, e, nt_)
-            piece = zs.at[base + peer * near + there - h * near]
+            peer, k = (t + 1 - 2 * parity, 1 - parity) if e else (t, parity)
+            piece = zs.at[base + k * near + there - h * near]
+            slot = rx3.at[parity, z]
 
             def remote():
-                send(piece, rx3.at[t, z], z2send, z2recv.at[t], {"z": there, "t": peer})
+                send(piece, slot, z2send, z2recv.at[parity], {"z": there, "t": peer})
 
             if i or e:
                 remote()
             else:
                 pl.when(there != z)(remote)
-                pl.when(there == z)(lambda: pltpu.make_async_copy(piece, rx3.at[t, z], z2recv.at[t]).start())
+                pl.when(there == z)(lambda: pltpu.make_async_copy(piece, slot, z2recv.at[parity]).start())
 
         for i in range(near):
-            for e in (2, 1, 3, 0):
+            for e in (1, 0):
                 give(i, e)
 
     for h in range(NG):
+        phase("zwait#h=%d" % h)
         take_z(h)
-    for h in range(NG):
-        take_y(h)
-        take_x(h, 0)
+    phase("yfwd#h=1")
+    take_y(1)
+    phase("xwait#h=0")
+    take_x(0)
+    phase("yfwd#h=2")
+    take_y(2)
+    take_y(3)
     phase("wwait")
     landed(wgu.at[1], wrecv.at[0])
     landed(wd.at[1], wrecv.at[1])
     landed(wsd.at[partner], wrecv.at[2])
-    take_x(0, 1)
-    take_x(1, 1)
     take_c(0)
     compute(0)
-    take_x(2, 1)
+    send_c(0)
+    sum_c(0)
+    phase("xwait#h=1")
+    take_x(1)
     take_c(1)
     compute(1)
-    sum_c(0)
-    take_x(3, 1)
+    send_c(1)
+    phase("xwait#h=2")
+    take_x(2)
+    sum_c(1)
     take_c(2)
     compute(2)
-    sum_c(1)
+    send_c(2)
+    sum_x(0)
+    phase("xwait#h=3")
+    take_x(3)
+    sum_c(2)
     take_c(3)
     compute(3)
-    sum_c(2)
+    send_c(3)
+    sum_x(1)
     sum_c(3)
-    for h in range(NG):
+    for h in (2, 3):
         sum_x(h)
     phase("z2wait")
-    for e in range(nt_):
-        k = idx(t, e, nt_)
-        landed(rx3.at[k], z2recv.at[k])
+    for p in (0, 1):
+        landed(rx3.at[p], z2recv.at[p])
     phase("result")
-    sums = [jnp.sum(rx3[k].astype(F32), axis=0) for k in range(nt_)]
-    out[...] = mine8 + jnp.concatenate(sums, axis=0)
+    sums = [jnp.sum(rx3[p].astype(F32), axis=0) for p in (0, 1)]
+    out[...] = mine8 + jnp.concatenate([sums[p][q] for q in (0, 1) for p in (0, 1)], axis=0)
 
     phase("drain")
     landed(pt.at[1:nt_], tsend)
-    landed(zb.at[1:nz], zsend)
+
+    @pl.when(group == 0)
+    def _():
+        pl.when(c == 0)(lambda: landed(zb, zsend))
+        pl.when(c == 1)(lambda: landed(zb.at[1:nz], zsend))
+
+    @pl.when(group != 0)
+    def _():
+        pl.when(c == 0)(lambda: landed(zb.at[:, 0], zsend))
+        pl.when(c == 1)(lambda: landed(zb.at[1:nz, 0], zsend))
+
     landed(wgu.at[0], wsend.at[0])
     landed(wd.at[0], wsend.at[1])
     landed(wsd.at[0], wsend.at[2])
-    landed(g.at[0, 0, 0:NG], ysend)
-    landed(zs.at[1 : nt_ * nz], z2send)
+
+    @pl.when(c == 1)
+    def _():
+        landed(g.at[0, 1:NG], ysend)
+        for h in range(NG):
+            landed(g.at[h, 2 : 2 * nx], xsend.at[h])
+            landed(g.at[h], csend.at[h])
+
+    landed(zs.at[1 : 2 * nz], z2send)
     for h in range(NG):
-        landed(g.at[h, 0, 2 : 2 * nx], xsend.at[h])
-        landed(g.at[h, 0], csend.at[h])
         landed(rx1.at[h], c2send.at[h])
         landed(rx2.at[h, 1 : 2 * nx], x2send.at[h])
     phase.close()
@@ -471,20 +544,21 @@
         pltpu.VMEM((2, depth, 2 * hidden), BF),
         pltpu.VMEM((2, hidden, depth), BF),
         pltpu.VMEM((ny, batch, depth), BF),
-        pltpu.VMEM((1, rows, depth + META), BF),
-        pltpu.VMEM((nz, rows, depth + META), BF),
-        pltpu.VMEM((NG, nc, 2 * nx, strip, depth + META), BF),
-        pltpu.VMEM((NG, nc, 2 * nx, strip, depth), BF),
-        pltpu.VMEM((NG, 2 * nx, strip, depth), BF),
-        pltpu.VMEM((NG, 2 * nx, strip, depth), BF),
-        pltpu.VMEM((NG, 2 * nx, strip, depth), BF),
-        pltpu.VMEM((ny * nz, rows, width), BF),
-        pltpu.VMEM((ny, nz, rows, width), BF),
+        pltpu.VMEM((2, rows, depth + META), BF),
+        pltpu.VMEM((nz // NG, nc, 2, rows, depth + META), BF),
+        pltpu.VMEM((nz, nc, rows, depth + META), BF),
+        pltpu.VMEM((NG, 2 * nx, nc, strip, depth + META), BF),
+        pltpu.VMEM((NG, nc, 2, nx, 2 * strip, depth // 2), BF),
+        pltpu.VMEM((NG, 2, nx, 2 * strip, depth // 2), BF),
+        pltpu.VMEM((NG, 2, nx, 2 * strip, depth // 2), BF),
+        pltpu.VMEM((NG, 2 * nx, 2 * strip, depth // 2), BF),
+        pltpu.VMEM((2 * nz, 2, rows, width), BF),
+        pltpu.VMEM((2, nz, 2, rows, width), BF),
         pltpu.SemaphoreType.REGULAR,
         dma((24,)),
         dma((3,)), dma((3,)),
-        dma, dma, dma, dma((NG,)), dma((NG,)), dma((NG, 2)), dma((NG,)), dma((NG,)), dma, dma((NG,)),
-        dma((NG,)), dma((NG,)), dma((NG,)), dma((NG,)), dma, dma((ny,)),
+        dma, dma, dma, dma((NG,)), dma((NG,)), dma((NG,)), dma((NG,)), dma((NG,)), dma, dma((NG,)),
+        dma((NG,)), dma((NG,)), dma((NG,)), dma((NG,)), dma, dma((2,)),
     ]
     return pl.pallas_call(
         functools.partial(kernel, dims),

time: 51.4 us -> 50.2 us (0.977)
  Pallas kernels: 48.8 us -> 48 us
    pallas_call x1, Pallas kernels: 48.8 us -> 48 us  [per_device(): pl.pallas_call(functools.partial(kernel, dims), out_shape=jax.ShapeDtypeS...]
where the time goes in v2:
time: 50.2 us; the launch traced here: 49.9 us
  Pallas kernels  48 us (96%)
  other arithmetic  1.29 us (3%)
  between operations  0.66 us (1%)
    pallas_call x1, Pallas kernels, per_device(): pl.pallas_call(functools.partial(kernel, dims), out_shape=jax.ShapeDtypeS...  48 us
    convert_element_type x1, other arithmetic, per_device(): return pl.pallas_call(functools.partial(kernel, dims), out_shape=jax.Shap...  1.29 us

profile of v2, /device:TPU:1, one launch (start us, length us, event | category | flops | bytes accessed | tf_op | source)
XLA Modules:
  0.0 49.9 jit_solution(92768540462228180)
XLA Ops:
  0.7 48.0 %shard_map.226 = f32[8,256]{1,0:T(8,128)} custom-call(bf16[8,1024]{1,0:T(8,128)(2,1)} %tokens_h.1, s32[8]{0:T(128)} %lengths_h.1, f32[8,1,512]{2,1,0:T(1,128)} %cum_h.1, bf16[1024]{0:T(1024)(128)(2,1)} %norm_gain_h.1, bf16[1,1024]{1,0:T(2,128)(2,1)} %bitcast.19, f32[1,1]{1,0:T(1,128)} %bitcast.11.forget_b_h, bf16[128]{0:T(256)(128)(2,1)} %query_gain_h.1, ...), custom_call_target="tpu_custom_call" | custom-call | tf_op jit(solution)/shard_map/pallas_call | solution.py:563
  48.6 1.3 %convert_element_type.3 = bf16[8,256]{1,0:T(8,128)(2,1)} convert(f32[8,256]{1,0:T(8,128)} %shard_map.226) | non-fusion elementwise | flops 2048 | bytes 12288 | tf_op jit(solution)/shard_map/convert_element_type | solution.py:578

commit v3 on v2

--- a/solution.py
+++ b/solution.py
@@ -336,10 +336,10 @@
         for dx in (2, 1, 3):
             for dq in (0, 1):
                 piece = g.at[h, spot(0, dq)]
-                send(piece, piece, xsend.at[h], xrecv.at[h], at("x", x, dx, nx))
+                send(piece, piece, xsend, xrecv.at[h, 1 if dx == 2 else 0], at("x", x, dx, nx))
         for dq in (0, 1):
             piece = g.at[h, spot(0, dq)]
-            send(piece, piece, csend.at[h], crecv.at[h], {"c": 0})
+            send(piece, piece, csend, crecv.at[h], {"c": 0})
 
     @core1
     def take_y(h):
@@ -348,11 +348,12 @@
 
     @core1
     def take_x(h):
-        landed(g.at[h, 2 : 2 * nx], xrecv.at[h])
-        for dx in range(1, nx):
-            for dq in (0, 1):
-                piece = g.at[h, spot(dx, dq)]
-                send(piece, piece, csend.at[h], crecv.at[h], {"c": 0})
+        for i, steps in enumerate(((1, 3), (2,))):
+            landed(g.at[h, 0 : 2 * len(steps)], xrecv.at[h, i])
+            for dx in steps:
+                for dq in (0, 1):
+                    piece = g.at[h, spot(dx, dq)]
+                    send(piece, piece, csend, crecv.at[h], {"c": 0})
 
     def take_c(h):
         phase("cwait#h=%d" % h)
@@ -383,7 +384,7 @@
                 p3[h, core, q] = value[:, core, :, q * side : (q + 1) * side].reshape(nx, 2 * strip, side).astype(BF)
 
     def send_c(h):
-        send(p3.at[h, 1 - c], rx1.at[h], c2send.at[h], c2recv.at[h], twin)
+        send(p3.at[h, 1 - c], rx1.at[h], c2send, c2recv.at[h], twin)
 
     def sum_c(h):
         phase("c2#h=%d" % h)
@@ -391,7 +392,7 @@
         for dx, dq in far_first:
             px, q = idx(x, dx, nx), 1 - level if dq else level
             s1[h, q, px] = (p3[h, c, q, px].astype(F32) + rx1[h, q, px].astype(F32)).astype(BF)
-            send(s1.at[h, q, px], rx2.at[h, 2 * dx + dq], x2send.at[h], x2recv.at[h], place_of(dx, dq))
+            send(s1.at[h, q, px], rx2.at[h, 2 * dx + dq], x2send, x2recv.at[h], place_of(dx, dq))
 
     def sum_x(h):
         phase("x2#h=%d" % h)
@@ -435,7 +436,6 @@
     take_x(0)
     phase("yfwd#h=2")
     take_y(2)
-    take_y(3)
     phase("wwait")
     landed(wgu.at[1], wrecv.at[0])
     landed(wd.at[1], wrecv.at[1])
@@ -444,6 +444,8 @@
     compute(0)
     send_c(0)
     sum_c(0)
+    phase("yfwd#h=3")
+    take_y(3)
     phase("xwait#h=1")
     take_x(1)
     take_c(1)
@@ -493,14 +495,12 @@
     @pl.when(c == 1)
     def _():
         landed(g.at[0, 1:NG], ysend)
-        for h in range(NG):
-            landed(g.at[h, 2 : 2 * nx], xsend.at[h])
-            landed(g.at[h], csend.at[h])
+        landed(g.at[:, 2 : 2 * nx], xsend)
+        landed(g, csend)
 
     landed(zs.at[1 : 2 * nz], z2send)
-    for h in range(NG):
-        landed(rx1.at[h], c2send.at[h])
-        landed(rx2.at[h, 1 : 2 * nx], x2send.at[h])
+    landed(rx1, c2send)
+    landed(rx2.at[:, 1 : 2 * nx], x2send)
     phase.close()
 
 
@@ -557,8 +557,8 @@
         pltpu.SemaphoreType.REGULAR,
         dma((24,)),
         dma((3,)), dma((3,)),
-        dma, dma, dma, dma((NG,)), dma((NG,)), dma((NG,)), dma((NG,)), dma((NG,)), dma, dma((NG,)),
-        dma((NG,)), dma((NG,)), dma((NG,)), dma((NG,)), dma, dma((2,)),
+        dma, dma, dma, dma((NG,)), dma, dma((NG, 2)), dma, dma((NG,)), dma, dma((NG,)),
+        dma, dma((NG,)), dma, dma((NG,)), dma, dma((2,)),
     ]
     return pl.pallas_call(
         functools.partial(kernel, dims),

time: 50.2 us -> 48.8 us (0.972)
  Pallas kernels: 48 us -> 46.6 us
    pallas_call x1, Pallas kernels: 48 us -> 46.6 us  [per_device(): pl.pallas_call(functools.partial(kernel, dims), out_shape=jax.ShapeDtypeS...]
where the time goes in v3:
time: 48.8 us; the launch traced here: 48.5 us
  Pallas kernels  46.6 us (95%)
  other arithmetic  1.29 us (3%)
  between operations  0.66 us (1%)
    pallas_call x1, Pallas kernels, per_device(): pl.pallas_call(functools.partial(kernel, dims), out_shape=jax.ShapeDtypeS...  46.6 us
    convert_element_type x1, other arithmetic, per_device(): return pl.pallas_call(functools.partial(kernel, dims), out_shape=jax.Shap...  1.29 us

profile of v3, /device:TPU:1, one launch (start us, length us, event | category | flops | bytes accessed | tf_op | source)
XLA Modules:
  0.0 48.5 jit_solution(13513749905580209936)
XLA Ops:
  0.7 46.6 %shard_map.226 = f32[8,256]{1,0:T(8,128)} custom-call(bf16[8,1024]{1,0:T(8,128)(2,1)} %tokens_h.1, s32[8]{0:T(128)} %lengths_h.1, f32[8,1,512]{2,1,0:T(1,128)} %cum_h.1, bf16[1024]{0:T(1024)(128)(2,1)} %norm_gain_h.1, bf16[1,1024]{1,0:T(2,128)(2,1)} %bitcast.19, f32[1,1]{1,0:T(1,128)} %bitcast.11.forget_b_h, bf16[128]{0:T(256)(128)(2,1)} %query_gain_h.1, ...), custom_call_target="tpu_custom_call" | custom-call | tf_op jit(solution)/shard_map/pallas_call | solution.py:563
  47.2 1.3 %convert_element_type.3 = bf16[8,256]{1,0:T(8,128)(2,1)} convert(f32[8,256]{1,0:T(8,128)} %shard_map.226) | non-fusion elementwise | flops 2048 | bytes 12288 | tf_op jit(solution)/shard_map/convert_element_type | solution.py:578
